TPU v7x, 32 devices: a whole 2x2x4 slice. The times are simulated.
32 devices in a mesh: sp: 16 (over z, y, core), tp: 2 (over x).
Axes of the slice: x: 2, y: 2, z: 4, core: 2. Of those that a mesh axis runs over, the one named last changes fastest.
Arguments:
- tokens: bfloat16 [8192, 2048], P(('sp', 'tp')), may hold values from -6 to 6
- norm_gain: float32 [2048], replicated, may hold values from 0.1 to 1.9
- query_weight: bfloat16 [2048, 1024], P(None, 'tp'), may hold values from -0.13258252 to 0.13258252
- key_weight: bfloat16 [2048, 1024], P(None, 'tp'), may hold values from -0.13258252 to 0.13258252
- value_weight: bfloat16 [2048, 1024], P(None, 'tp'), may hold values from -0.125 to 0.125
- glu_value_weight: bfloat16 [2048, 1024], P(None, 'tp'), may hold values from -0.125 to 0.125
- glu_gate_weight: bfloat16 [2048, 1024], P(None, 'tp'), may hold values from -0.125 to 0.125
- qk_gain: float32 [2, 64], replicated, may hold values from 1 to 6
- mix_lambda: float32 [8], P('tp'), may hold values from 0.3 to 0.8
- head_gain: float32 [128], replicated, may hold values from 0.1 to 1.9
- conv_kernel: float32 [31, 1024], P(None, 'tp'), may hold values from -1 to 1
- channel_gain: float32 [1024], P('tp'), may hold values from 0.1 to 1.9
- channel_shift: float32 [1024], P('tp'), may hold values from -3 to 3
- output_weight: bfloat16 [2048, 2048], replicated, may hold values from -0.125 to 0.125
Outputs:
- mixed: bfloat16 [8192, 2048], P(('sp', 'tp'))
- log_totals: float32 [2, 8, 8192], P(None, 'tp', 'sp')
All inputs are finite; a program needn't handle non-finite values.
Results may differ from a plain program's by a relative error of at most 0.035.
Values may be sent and summed in bfloat16 or wider, within the bound.
A program may use at most 128 MiB of HBM per device.

v0:
```python
import math
import jax
import jax.numpy as jnp
from jax import lax
from jax.sharding import PartitionSpec as P


def from_behind(value, axis, steps):
    count = lax.axis_size(axis)
    leading, last = (max(0, -steps), min(count, count - steps))
    return lax.ppermute(value, axis, [(source, source + steps) for source in range(leading, last)])


def rotate(values, positions):
    half = values.shape[-1] // 2
    inverse = 10000.0 ** (-jnp.arange(0, half, dtype=jnp.float32) * 2.0 / values.shape[-1])
    angles = positions[:, None] * inverse[None, :]
    cosine = jnp.cos(angles)[:, None, None, :]
    sine = jnp.sin(angles)[:, None, None, :]
    first = values[..., :half]
    second = values[..., half:]
    return jnp.concatenate(
        [first * cosine - second * sine, second * cosine + first * sine], axis=-1
    )


def prepare(raw, qk_gain, positions):
    values = raw.astype(jnp.float32)
    values = values * lax.rsqrt(jnp.mean(values * values, axis=-1, keepdims=True) + 1e-06)
    values = values * qk_gain[None, None, :, :]
    return rotate(values, positions).astype(jnp.bfloat16)


def per_device(
    tokens,
    norm_gain,
    query_weight,
    key_weight,
    value_weight,
    glu_value_weight,
    glu_gate_weight,
    qk_gain,
    mix_lambda,
    head_gain,
    conv_kernel,
    channel_gain,
    channel_shift,
    output_weight,
):
    head_size = qk_gain.shape[1]
    heads_here = mix_lambda.shape[0]
    value_size = head_gain.shape[0]
    kernel_len = conv_kernel.shape[0]
    conv_here = conv_kernel.shape[1]
    width = tokens.shape[1]
    matrices = (query_weight, key_weight, value_weight, glu_value_weight, glu_gate_weight)

    def project(piece):
        inputs = piece.astype(jnp.float32)
        normed = (
            inputs
            * lax.rsqrt(jnp.mean(inputs * inputs, axis=-1, keepdims=True) + 1e-06)
            * norm_gain
        ).astype(jnp.bfloat16)
        results = [
            jnp.dot(normed, matrix, preferred_element_type=jnp.float32).astype(jnp.bfloat16)
            for matrix in matrices
        ]
        return jnp.concatenate(results, axis=1)

    projected = project(lax.all_gather(tokens, "tp", axis=0, tiled=True))
    tok_rows = projected.shape[0]
    bounds = [0]
    for matrix in matrices:
        bounds.append(bounds[-1] + matrix.shape[1])
    queries = projected[:, bounds[0] : bounds[1]].reshape(tok_rows, heads_here, 2, head_size)
    keys = projected[:, bounds[1] : bounds[2]].reshape(tok_rows, heads_here, 2, head_size)
    values = projected[:, bounds[2] : bounds[3]].reshape(tok_rows, heads_here, value_size)
    glu_a = projected[:, bounds[3] : bounds[4]]
    glu_g = projected[:, bounds[4] : bounds[5]]
    offset = lax.axis_index("sp") * tok_rows
    query_pos = offset + jnp.arange(tok_rows, dtype=jnp.int32)
    float_pos = query_pos.astype(jnp.float32)
    rq = jnp.transpose(prepare(queries, qk_gain, float_pos), (1, 2, 0, 3))
    rk = prepare(keys, qk_gain, float_pos)
    scale = head_size ** (-0.5)
    last_query = offset + tok_rows - 1
    initial = (
        jnp.full((heads_here, 2, tok_rows), -1e30, jnp.float32),
        jnp.zeros((heads_here, 2, tok_rows), jnp.float32),
        jnp.zeros((heads_here, 2, tok_rows, value_size), jnp.float32),
    )
    carry = initial
    key_piece = lax.all_gather(rk, "sp", axis=0, tiled=True)
    value_piece = lax.all_gather(values, "sp", axis=0, tiled=True)
    count = key_piece.shape[0]
    block = math.gcd(count, 512)
    blocks = count // block
    key_blocks = key_piece.reshape(blocks, block, heads_here, 2, head_size)
    value_blocks = value_piece.reshape(blocks, block, heads_here, value_size)

    def advance(state, item):
        key_block, value_block, number = item
        key_start = number * block

        def compute(inner):
            running, totals, summed = inner
            scores = (
                jnp.einsum("hmqd,khmd->hmqk", rq, key_block, preferred_element_type=jnp.float32)
                * scale
            )
            key_pos = key_start + jnp.arange(block, dtype=jnp.int32)
            allowed = key_pos[None, :] <= query_pos[:, None]
            scores = jnp.where(allowed[None, None], scores, -1e30)
            newtop = jnp.maximum(running, jnp.max(scores, axis=-1))
            probs = jnp.where(allowed[None, None], jnp.exp(scores - newtop[..., None]), 0.0)
            factor = jnp.exp(running - newtop)
            totals = totals * factor + jnp.sum(probs, axis=-1)
            added = jnp.einsum(
                "hmqk,khd->hmqd",
                probs.astype(jnp.bfloat16),
                value_block,
                preferred_element_type=jnp.float32,
            )
            return (newtop, totals, summed * factor[..., None] + added)

        def keep(inner):
            return inner

        return (lax.cond(key_start <= last_query, compute, keep, state), None)

    carry, unused = lax.scan(
        advance, carry, (key_blocks, value_blocks, jnp.arange(blocks, dtype=jnp.int32))
    )
    running, totals, summed = carry
    heads_out = (
        summed[:, 0] / totals[:, 0, :, None]
        - mix_lambda[:, None, None] * summed[:, 1] / totals[:, 1, :, None]
    )
    heads_out = (
        heads_out
        * lax.rsqrt(jnp.mean(heads_out * heads_out, axis=-1, keepdims=True) + 1e-06)
        * head_gain
    )
    attended = jnp.transpose(heads_out.astype(jnp.bfloat16), (1, 0, 2)).reshape(
        tok_rows, heads_here * value_size
    )
    log_totals = jnp.transpose(running + jnp.log(totals), (1, 0, 2))
    gated = (glu_a.astype(jnp.float32) * jax.nn.sigmoid(glu_g.astype(jnp.float32))).astype(
        jnp.bfloat16
    )
    earlier = from_behind(gated[tok_rows - (kernel_len - 1) :], "sp", 1)
    extended = jnp.concatenate([earlier, gated], axis=0).astype(jnp.float32)
    convolved = jnp.zeros((tok_rows, conv_here), jnp.float32)
    for step in range(kernel_len):
        convolved = convolved + conv_kernel[step][None, :] * extended[step : step + tok_rows]
    plain_sum, square_sum = lax.psum(
        (jnp.sum(convolved, axis=1), jnp.sum(convolved * convolved, axis=1)), "tp"
    )
    channels = conv_here * lax.axis_size("tp")
    middle = (plain_sum / channels)[:, None]
    spread = (square_sum / channels)[:, None] - middle * middle
    conv_out = jax.nn.silu(
        (convolved - middle) * lax.rsqrt(spread + 1e-05) * channel_gain + channel_shift
    ).astype(jnp.bfloat16)
    merged = jnp.concatenate([attended, conv_out], axis=1)
    groups = lax.axis_size("tp")
    branch_width = heads_here * value_size
    weight_view = output_weight.reshape(2, groups, branch_width, width)
    moved = lax.all_to_all(merged, "tp", split_axis=0, concat_axis=1, tiled=True)
    arranged = moved.reshape(tok_rows // groups, groups, 2, branch_width)
    mixed = jnp.einsum(
        "rtcj,ctjd->rd", arranged, weight_view, preferred_element_type=jnp.float32
    ).astype(jnp.bfloat16)
    return (mixed, log_totals)


def solution(mesh):
    placed = (
        P(("sp", "tp"), None),
        P(),
        P(None, "tp"),
        P(None, "tp"),
        P(None, "tp"),
        P(None, "tp"),
        P(None, "tp"),
        P(),
        P("tp"),
        P(),
        P(None, "tp"),
        P("tp"),
        P("tp"),
        P(),
    )
    return jax.shard_map(
        per_device,
        mesh=mesh,
        in_specs=placed,
        out_specs=(P(("sp", "tp"), None), P(None, "tp", "sp")),
        check_vma=False,
    )
```

profile of v0, /device:TPU:29, one launch (start us, length us, event | category | flops | bytes accessed | tf_op | source)
XLA Modules:
  0.0 434.6 jit_solution(18231954651570132200)
XLA Ops:
  8.0 35.5 %all-gather.4.cloned.1.call-done = bf16[512,2048]{1,0:T(8,128)(2,1)} async-done(((bf16[256,2048]{1,0:T(8,128)(2,1)}), bf16[512,2048]{1,0:T(8,128)(2,1)}) %all-gather.4.cloned.1.call-update) | async-done | bytes 2097168 | tf_op jit(solution)/shard_map/all_gather | solution.py:71
  65.7 5.0 %fusion.77 = (f32[512]{0:T(512)S(1)}, f32[512]{0:T(512)S(1)}, f32[512,512]{1,0:T(8,128)S(1)}) fusion(f32[542,512]{1,0:T(8,128)S(1)} %maximum_convert_fusion, f32[512]{0:T(512)S(1)} %bitcast.147, f32[512]{0:T(512)S(1)} %bitcast.148, f32[512]{0:T(512)S(1)} %bitcast.150, f32[512]{0:T(512)S(1)} %bitcast.151, f32[512]{0:T(512)S(1)} %bitcast.152, ...), kind=kLoop, calls=%fused_computation.148 | loop fusion | flops 16776192 | bytes 33622016 | tf_op jit(solution)/shard_map/reduce_sum | solution.py:158
  75.5 47.3 %all-gather.8.cloned.1.call-done = bf16[8192,4,128]{2,0,1:T(8,128)(2,1)} async-done(((bf16[512,4,128]{2,0,1:T(8,128)(2,1)}), bf16[8192,4,128]{2,0,1:T(8,128)(2,1)}) %all-gather.8.cloned.1.call-update) | async-done | bytes 8388624 | tf_op jit(solution)/shard_map/all_gather | solution.py:95
  122.8 7.6 %copy.23 = bf16[16,512,4,128]{3,1,2,0:T(8,128)(2,1)} copy(bf16[16,512,4,128]{3,1,0,2:T(8,128)(2,1)} %bitcast.123) | data formatting | bytes 16777216
  130.4 71.0 %all-gather.6.cloned.1.call-done = bf16[8192,4,2,64]{0,3,2,1:T(8,128)(2,1)} async-done(((bf16[512,4,2,64]{0,3,2,1:T(8,128)(2,1)}), bf16[8192,4,2,64]{0,3,2,1:T(8,128)(2,1)}) %all-gather.6.cloned.1.call-update) | async-done | bytes 8388624 | tf_op jit(solution)/shard_map/all_gather | solution.py:94
  201.4 7.9 %copy.51 = bf16[4,2,8,16,8,512]{5,4,2,1,0,3:T(8,128)(2,1)} copy(bf16[4,2,8,16,8,512]{5,4,3,2,1,0:T(8,128)(2,1)} %bitcast.124) | data formatting | bytes 16777216 | tf_op jit(solution)/shard_map/reshape | solution.py:99
  210.8 193.6 %while.15 = (s32[]{:T(128)}, f32[4,2,512]{2,1,0:T(2,128)S(1)}, f32[4,2,512]{2,1,0:T(2,128)S(1)}, f32[4,2,512,128]{3,2,1,0:T(8,128)}, s32[16]{0:T(128)S(1)}, /*in...) while((s32[]{:T(128)}, f32[4,2,512]{2,1,0:T(2,128)S(1)}, ...), condition=%wide.region_8.9_spmd.clone, body=%wide.region_3.8_spmd.clone.sunk | while | flops 833889280 | bytes 49034600 | solution.py:132
  212.1 10.8 %conditional.3 = ((f32[4,2,512]{2,1,0:T(2,128)S(1)}, f32[4,2,512]{2,1,0:T(2,128)S(1)}, f32[4,2,512,128]{3,2,1,0:T(8,128)})) conditional(s32[]{:T(128)} %convert_element_type.168, (f32[4,2,512]{2,1,0:T(2,128)S(1)}, f32[4,2,512]{2,1,0:T(2,128)S(1)}, f32[4,2,512,128]{3,2,1,0:T(8,128)}) %tuple.88, (s32[]{:T(128)}, s32[]{:T(128)}, ...), branch_computations={%region_4.4_spmd, %region_5.7_spmd} | conditional | flops 833889280 | bytes 49032288 | solution.py:130
  217.0 4.6 %multiply_add_fusion = f32[4,2,512,128]{3,2,1,0:T(8,128)S(1)} fusion(f32[4,2,512,128]{3,2,1,0:T(8,128)S(1)} %copy-done.2, f32[4,2,512,512]{3,2,1,0:T(8,128)S(1)} %get-tuple-element.211, f32[4,2,512]{2,1,0:T(2,128)S(1)} %max.4, pred[512,512]{0,1:T(8,128)(4,1)S(1)} %broadcast_compare_fusion, f32[4,2,512]{2,1,0:T(2,128)S(1)} %bitcast.134, ...), kind=kOutput, calls=%fused_computation.8 | convolution fusion | flops 548405248 | bytes 13402624 | tf_op jit(solution)/shard_map/while/body/eval_jaxpr/cond/branch_1_fun/hmqk,khd->hmqd/dot_general | solution.py:119
  224.2 10.8 %conditional.3 = ((f32[4,2,512]{2,1,0:T(2,128)S(1)}, f32[4,2,512]{2,1,0:T(2,128)S(1)}, f32[4,2,512,128]{3,2,1,0:T(8,128)})) conditional(s32[]{:T(128)} %convert_element_type.168, (f32[4,2,512]{2,1,0:T(2,128)S(1)}, f32[4,2,512]{2,1,0:T(2,128)S(1)}, f32[4,2,512,128]{3,2,1,0:T(8,128)}) %tuple.88, (s32[]{:T(128)}, s32[]{:T(128)}, ...), branch_computations={%region_4.4_spmd, %region_5.7_spmd} | conditional | flops 833889280 | bytes 49032288 | solution.py:130
  229.1 4.6 %multiply_add_fusion = f32[4,2,512,128]{3,2,1,0:T(8,128)S(1)} fusion(f32[4,2,512,128]{3,2,1,0:T(8,128)S(1)} %copy-done.2, f32[4,2,512,512]{3,2,1,0:T(8,128)S(1)} %get-tuple-element.211, f32[4,2,512]{2,1,0:T(2,128)S(1)} %max.4, pred[512,512]{0,1:T(8,128)(4,1)S(1)} %broadcast_compare_fusion, f32[4,2,512]{2,1,0:T(2,128)S(1)} %bitcast.134, ...), kind=kOutput, calls=%fused_computation.8 | convolution fusion | flops 548405248 | bytes 13402624 | tf_op jit(solution)/shard_map/while/body/eval_jaxpr/cond/branch_1_fun/hmqk,khd->hmqd/dot_general | solution.py:119
  236.3 10.8 %conditional.3 = ((f32[4,2,512]{2,1,0:T(2,128)S(1)}, f32[4,2,512]{2,1,0:T(2,128)S(1)}, f32[4,2,512,128]{3,2,1,0:T(8,128)})) conditional(s32[]{:T(128)} %convert_element_type.168, (f32[4,2,512]{2,1,0:T(2,128)S(1)}, f32[4,2,512]{2,1,0:T(2,128)S(1)}, f32[4,2,512,128]{3,2,1,0:T(8,128)}) %tuple.88, (s32[]{:T(128)}, s32[]{:T(128)}, ...), branch_computations={%region_4.4_spmd, %region_5.7_spmd} | conditional | flops 833889280 | bytes 49032288 | solution.py:130
  248.4 10.8 %conditional.3 = ((f32[4,2,512]{2,1,0:T(2,128)S(1)}, f32[4,2,512]{2,1,0:T(2,128)S(1)}, f32[4,2,512,128]{3,2,1,0:T(8,128)})) conditional(s32[]{:T(128)} %convert_element_type.168, (f32[4,2,512]{2,1,0:T(2,128)S(1)}, f32[4,2,512]{2,1,0:T(2,128)S(1)}, f32[4,2,512,128]{3,2,1,0:T(8,128)}) %tuple.88, (s32[]{:T(128)}, s32[]{:T(128)}, ...), branch_computations={%region_4.4_spmd, %region_5.7_spmd} | conditional | flops 833889280 | bytes 49032288 | solution.py:130
  253.3 4.6 %multiply_add_fusion = f32[4,2,512,128]{3,2,1,0:T(8,128)S(1)} fusion(f32[4,2,512,128]{3,2,1,0:T(8,128)S(1)} %copy-done.2, f32[4,2,512,512]{3,2,1,0:T(8,128)S(1)} %get-tuple-element.211, f32[4,2,512]{2,1,0:T(2,128)S(1)} %max.4, pred[512,512]{0,1:T(8,128)(4,1)S(1)} %broadcast_compare_fusion, f32[4,2,512]{2,1,0:T(2,128)S(1)} %bitcast.134, ...), kind=kOutput, calls=%fused_computation.8 | convolution fusion | flops 548405248 | bytes 13402624 | tf_op jit(solution)/shard_map/while/body/eval_jaxpr/cond/branch_1_fun/hmqk,khd->hmqd/dot_general | solution.py:119
  260.5 10.8 %conditional.3 = ((f32[4,2,512]{2,1,0:T(2,128)S(1)}, f32[4,2,512]{2,1,0:T(2,128)S(1)}, f32[4,2,512,128]{3,2,1,0:T(8,128)})) conditional(s32[]{:T(128)} %convert_element_type.168, (f32[4,2,512]{2,1,0:T(2,128)S(1)}, f32[4,2,512]{2,1,0:T(2,128)S(1)}, f32[4,2,512,128]{3,2,1,0:T(8,128)}) %tuple.88, (s32[]{:T(128)}, s32[]{:T(128)}, ...), branch_computations={%region_4.4_spmd, %region_5.7_spmd} | conditional | flops 833889280 | bytes 49032288 | solution.py:130
  272.6 10.8 %conditional.3 = ((f32[4,2,512]{2,1,0:T(2,128)S(1)}, f32[4,2,512]{2,1,0:T(2,128)S(1)}, f32[4,2,512,128]{3,2,1,0:T(8,128)})) conditional(s32[]{:T(128)} %convert_element_type.168, (f32[4,2,512]{2,1,0:T(2,128)S(1)}, f32[4,2,512]{2,1,0:T(2,128)S(1)}, f32[4,2,512,128]{3,2,1,0:T(8,128)}) %tuple.88, (s32[]{:T(128)}, s32[]{:T(128)}, ...), branch_computations={%region_4.4_spmd, %region_5.7_spmd} | conditional | flops 833889280 | bytes 49032288 | solution.py:130
  284.7 10.8 %conditional.3 = ((f32[4,2,512]{2,1,0:T(2,128)S(1)}, f32[4,2,512]{2,1,0:T(2,128)S(1)}, f32[4,2,512,128]{3,2,1,0:T(8,128)})) conditional(s32[]{:T(128)} %convert_element_type.168, (f32[4,2,512]{2,1,0:T(2,128)S(1)}, f32[4,2,512]{2,1,0:T(2,128)S(1)}, f32[4,2,512,128]{3,2,1,0:T(8,128)}) %tuple.88, (s32[]{:T(128)}, s32[]{:T(128)}, ...), branch_computations={%region_4.4_spmd, %region_5.7_spmd} | conditional | flops 833889280 | bytes 49032288 | solution.py:130
  289.6 4.6 %multiply_add_fusion = f32[4,2,512,128]{3,2,1,0:T(8,128)S(1)} fusion(f32[4,2,512,128]{3,2,1,0:T(8,128)S(1)} %copy-done.2, f32[4,2,512,512]{3,2,1,0:T(8,128)S(1)} %get-tuple-element.211, f32[4,2,512]{2,1,0:T(2,128)S(1)} %max.4, pred[512,512]{0,1:T(8,128)(4,1)S(1)} %broadcast_compare_fusion, f32[4,2,512]{2,1,0:T(2,128)S(1)} %bitcast.134, ...), kind=kOutput, calls=%fused_computation.8 | convolution fusion | flops 548405248 | bytes 13402624 | tf_op jit(solution)/shard_map/while/body/eval_jaxpr/cond/branch_1_fun/hmqk,khd->hmqd/dot_general | solution.py:119
  296.8 10.8 %conditional.3 = ((f32[4,2,512]{2,1,0:T(2,128)S(1)}, f32[4,2,512]{2,1,0:T(2,128)S(1)}, f32[4,2,512,128]{3,2,1,0:T(8,128)})) conditional(s32[]{:T(128)} %convert_element_type.168, (f32[4,2,512]{2,1,0:T(2,128)S(1)}, f32[4,2,512]{2,1,0:T(2,128)S(1)}, f32[4,2,512,128]{3,2,1,0:T(8,128)}) %tuple.88, (s32[]{:T(128)}, s32[]{:T(128)}, ...), branch_computations={%region_4.4_spmd, %region_5.7_spmd} | conditional | flops 833889280 | bytes 49032288 | solution.py:130
  308.9 10.8 %conditional.3 = ((f32[4,2,512]{2,1,0:T(2,128)S(1)}, f32[4,2,512]{2,1,0:T(2,128)S(1)}, f32[4,2,512,128]{3,2,1,0:T(8,128)})) conditional(s32[]{:T(128)} %convert_element_type.168, (f32[4,2,512]{2,1,0:T(2,128)S(1)}, f32[4,2,512]{2,1,0:T(2,128)S(1)}, f32[4,2,512,128]{3,2,1,0:T(8,128)}) %tuple.88, (s32[]{:T(128)}, s32[]{:T(128)}, ...), branch_computations={%region_4.4_spmd, %region_5.7_spmd} | conditional | flops 833889280 | bytes 49032288 | solution.py:130
  313.8 4.6 %multiply_add_fusion = f32[4,2,512,128]{3,2,1,0:T(8,128)S(1)} fusion(f32[4,2,512,128]{3,2,1,0:T(8,128)S(1)} %copy-done.2, f32[4,2,512,512]{3,2,1,0:T(8,128)S(1)} %get-tuple-element.211, f32[4,2,512]{2,1,0:T(2,128)S(1)} %max.4, pred[512,512]{0,1:T(8,128)(4,1)S(1)} %broadcast_compare_fusion, f32[4,2,512]{2,1,0:T(2,128)S(1)} %bitcast.134, ...), kind=kOutput, calls=%fused_computation.8 | convolution fusion | flops 548405248 | bytes 13402624 | tf_op jit(solution)/shard_map/while/body/eval_jaxpr/cond/branch_1_fun/hmqk,khd->hmqd/dot_general | solution.py:119
  321.0 10.8 %conditional.3 = ((f32[4,2,512]{2,1,0:T(2,128)S(1)}, f32[4,2,512]{2,1,0:T(2,128)S(1)}, f32[4,2,512,128]{3,2,1,0:T(8,128)})) conditional(s32[]{:T(128)} %convert_element_type.168, (f32[4,2,512]{2,1,0:T(2,128)S(1)}, f32[4,2,512]{2,1,0:T(2,128)S(1)}, f32[4,2,512,128]{3,2,1,0:T(8,128)}) %tuple.88, (s32[]{:T(128)}, s32[]{:T(128)}, ...), branch_computations={%region_4.4_spmd, %region_5.7_spmd} | conditional | flops 833889280 | bytes 49032288 | solution.py:130
  333.1 10.8 %conditional.3 = ((f32[4,2,512]{2,1,0:T(2,128)S(1)}, f32[4,2,512]{2,1,0:T(2,128)S(1)}, f32[4,2,512,128]{3,2,1,0:T(8,128)})) conditional(s32[]{:T(128)} %convert_element_type.168, (f32[4,2,512]{2,1,0:T(2,128)S(1)}, f32[4,2,512]{2,1,0:T(2,128)S(1)}, f32[4,2,512,128]{3,2,1,0:T(8,128)}) %tuple.88, (s32[]{:T(128)}, s32[]{:T(128)}, ...), branch_computations={%region_4.4_spmd, %region_5.7_spmd} | conditional | flops 833889280 | bytes 49032288 | solution.py:130
  345.2 10.8 %conditional.3 = ((f32[4,2,512]{2,1,0:T(2,128)S(1)}, f32[4,2,512]{2,1,0:T(2,128)S(1)}, f32[4,2,512,128]{3,2,1,0:T(8,128)})) conditional(s32[]{:T(128)} %convert_element_type.168, (f32[4,2,512]{2,1,0:T(2,128)S(1)}, f32[4,2,512]{2,1,0:T(2,128)S(1)}, f32[4,2,512,128]{3,2,1,0:T(8,128)}) %tuple.88, (s32[]{:T(128)}, s32[]{:T(128)}, ...), branch_computations={%region_4.4_spmd, %region_5.7_spmd} | conditional | flops 833889280 | bytes 49032288 | solution.py:130
  350.1 4.6 %multiply_add_fusion = f32[4,2,512,128]{3,2,1,0:T(8,128)S(1)} fusion(f32[4,2,512,128]{3,2,1,0:T(8,128)S(1)} %copy-done.2, f32[4,2,512,512]{3,2,1,0:T(8,128)S(1)} %get-tuple-element.211, f32[4,2,512]{2,1,0:T(2,128)S(1)} %max.4, pred[512,512]{0,1:T(8,128)(4,1)S(1)} %broadcast_compare_fusion, f32[4,2,512]{2,1,0:T(2,128)S(1)} %bitcast.134, ...), kind=kOutput, calls=%fused_computation.8 | convolution fusion | flops 548405248 | bytes 13402624 | tf_op jit(solution)/shard_map/while/body/eval_jaxpr/cond/branch_1_fun/hmqk,khd->hmqd/dot_general | solution.py:119
  357.3 10.8 %conditional.3 = ((f32[4,2,512]{2,1,0:T(2,128)S(1)}, f32[4,2,512]{2,1,0:T(2,128)S(1)}, f32[4,2,512,128]{3,2,1,0:T(8,128)})) conditional(s32[]{:T(128)} %convert_element_type.168, (f32[4,2,512]{2,1,0:T(2,128)S(1)}, f32[4,2,512]{2,1,0:T(2,128)S(1)}, f32[4,2,512,128]{3,2,1,0:T(8,128)}) %tuple.88, (s32[]{:T(128)}, s32[]{:T(128)}, ...), branch_computations={%region_4.4_spmd, %region_5.7_spmd} | conditional | flops 833889280 | bytes 49032288 | solution.py:130
  369.4 10.8 %conditional.3 = ((f32[4,2,512]{2,1,0:T(2,128)S(1)}, f32[4,2,512]{2,1,0:T(2,128)S(1)}, f32[4,2,512,128]{3,2,1,0:T(8,128)})) conditional(s32[]{:T(128)} %convert_element_type.168, (f32[4,2,512]{2,1,0:T(2,128)S(1)}, f32[4,2,512]{2,1,0:T(2,128)S(1)}, f32[4,2,512,128]{3,2,1,0:T(8,128)}) %tuple.88, (s32[]{:T(128)}, s32[]{:T(128)}, ...), branch_computations={%region_4.4_spmd, %region_5.7_spmd} | conditional | flops 833889280 | bytes 49032288 | solution.py:130
  381.5 10.8 %conditional.3 = ((f32[4,2,512]{2,1,0:T(2,128)S(1)}, f32[4,2,512]{2,1,0:T(2,128)S(1)}, f32[4,2,512,128]{3,2,1,0:T(8,128)})) conditional(s32[]{:T(128)} %convert_element_type.168, (f32[4,2,512]{2,1,0:T(2,128)S(1)}, f32[4,2,512]{2,1,0:T(2,128)S(1)}, f32[4,2,512,128]{3,2,1,0:T(8,128)}) %tuple.88, (s32[]{:T(128)}, s32[]{:T(128)}, ...), branch_computations={%region_4.4_spmd, %region_5.7_spmd} | conditional | flops 833889280 | bytes 49032288 | solution.py:130
  386.4 4.6 %multiply_add_fusion = f32[4,2,512,128]{3,2,1,0:T(8,128)S(1)} fusion(f32[4,2,512,128]{3,2,1,0:T(8,128)S(1)} %copy-done.2, f32[4,2,512,512]{3,2,1,0:T(8,128)S(1)} %get-tuple-element.211, f32[4,2,512]{2,1,0:T(2,128)S(1)} %max.4, pred[512,512]{0,1:T(8,128)(4,1)S(1)} %broadcast_compare_fusion, f32[4,2,512]{2,1,0:T(2,128)S(1)} %bitcast.134, ...), kind=kOutput, calls=%fused_computation.8 | convolution fusion | flops 548405248 | bytes 13402624 | tf_op jit(solution)/shard_map/while/body/eval_jaxpr/cond/branch_1_fun/hmqk,khd->hmqd/dot_general | solution.py:119
  393.6 10.8 %conditional.3 = ((f32[4,2,512]{2,1,0:T(2,128)S(1)}, f32[4,2,512]{2,1,0:T(2,128)S(1)}, f32[4,2,512,128]{3,2,1,0:T(8,128)})) conditional(s32[]{:T(128)} %convert_element_type.168, (f32[4,2,512]{2,1,0:T(2,128)S(1)}, f32[4,2,512]{2,1,0:T(2,128)S(1)}, f32[4,2,512,128]{3,2,1,0:T(8,128)}) %tuple.88, (s32[]{:T(128)}, s32[]{:T(128)}, ...), branch_computations={%region_4.4_spmd, %region_5.7_spmd} | conditional | flops 833889280 | bytes 49032288 | solution.py:130
  413.1 7.6 %all-to-all-done = bf16[2,256,1024]{2,1,0:T(8,128)(2,1)S(1)} async-done(((bf16[2,256,1024]{2,1,0:T(8,128)(2,1)}), bf16[2,256,1024]{2,1,0:T(8,128)(2,1)S(1)}, u32[]{:S(2)}, u32[]{:S(2)}) %all-to-all-start) | async-done | bytes 1048608 | tf_op jit(solution)/shard_map/all_to_all | solution.py:170
  421.2 6.8 %fusion.23 = bf16[256,2048]{1,0:T(8,128)(2,1)} fusion(bf16[2,2,512,2048]{3,2,1,0:T(8,128)(2,1)} %bitcast.122, bf16[256,2,2,512]{0,3,2,1:T(8,128)(2,1)S(1)} %bitcast.126), kind=kOutput, calls=%fused_computation.31 | convolution fusion | flops 2148007936 | bytes 10485760 | tf_op jit(solution)/shard_map/rtcj,ctjd->rd/dot_general | solution.py:172
  (292 shorter events, 187.9 us)
Async XLA Ops:
  7.2 43.0 %copy-start = (bf16[2048,512]{1,0:T(8,128)(2,1)S(1)}, bf16[2048,512]{1,0:T(8,128)(2,1)}, u32[]{:S(2)}) copy-start(bf16[2048,512]{1,0:T(8,128)(2,1)} %param.20) | copy-start | bytes 6291460
  7.2 38.5 %copy-start.15 = (f32[2048]{0:T(1024)S(1)}, f32[2048]{0:T(1024)}, u32[]{:S(2)}) copy-start(f32[2048]{0:T(1024)} %param.19) | copy-start | bytes 24580
  7.2 36.2 %all-gather.4.cloned.1.call-start = ((), (), s32[]{:S(2)}) async-start(), calls=%async_computation.1 | async-start | bytes 3145728 | tf_op jit(solution)/shard_map/all_gather | solution.py:71
  7.9 114.9 %all-gather.8.cloned.1.call-start = ((), (), s32[]{:S(2)}) async-start(), calls=%async_computation.3 | async-start | bytes 8912896 | tf_op jit(solution)/shard_map/all_gather | solution.py:95
  43.4 2.2 copy-start.4
  49.7 151.6 %all-gather.6.cloned.1.call-start = ((), (), s32[]{:S(2)}) async-start(), calls=%async_computation.2 | async-start | bytes 8912896 | tf_op jit(solution)/shard_map/all_gather | solution.py:94
  50.1 3.2 copy-start.5
  50.2 3.2 copy-start.13
  56.5 4.0 copy-start.6
  56.5 4.0 copy-start.14
  62.0 3.4 collective-permute-start
  65.6 9.4 %copy-start.8 = (f32[512]{0:T(512)S(1)}, f32[512]{0:T(512)}, u32[]{:S(2)}) copy-start(f32[512]{0:T(512)} %param.30) | copy-start | bytes 6148
  65.7 9.4 %copy-start.9 = (f32[512]{0:T(512)S(1)}, f32[512]{0:T(512)}, u32[]{:S(2)}) copy-start(f32[512]{0:T(512)} %param.29) | copy-start | bytes 6148
  210.8 193.7 %copy-start.12 = (f32[4]{0:T(128)S(1)}, f32[4]{0:T(128)}, u32[]{:S(2)}) copy-start(f32[4]{0:T(128)} %param.26) | copy-start | bytes 52
  214.9 2.1 copy-start.2
  227.0 2.1 copy-start.2
  239.1 2.1 copy-start.2
  251.2 2.1 copy-start.2
  263.3 2.1 copy-start.2
  275.4 2.1 copy-start.2
  287.5 2.1 copy-start.2
  299.6 2.1 copy-start.2
  311.7 2.1 copy-start.2
  323.8 2.1 copy-start.2
  335.9 2.1 copy-start.2
  348.0 2.1 copy-start.2
  360.1 2.1 copy-start.2
  372.2 2.1 copy-start.2
  384.3 2.1 copy-start.2
  404.4 2.3 copy-start.11
  408.9 11.8 %all-to-all-start = ((bf16[2,256,1024]{2,1,0:T(8,128)(2,1)}), bf16[2,256,1024]{2,1,0:T(8,128)(2,1)S(1)}, u32[]{:S(2)}, u32[]{:S(2)}) async-start(bf16[2,256,1024]{2,1,0:T(8,128)(2,1)} %pad_maximum_fusion), calls=%async_computation | async-start | bytes 2097152 | tf_op jit(solution)/shard_map/all_to_all | solution.py:170
  421.2 6.9 %copy-start.1 = (bf16[2048,512]{1,0:T(8,128)(2,1)S(1)}, bf16[2048,512]{1,0:T(8,128)(2,1)}, u32[]{:S(2)}) copy-start(bf16[2048,512]{1,0:T(8,128)(2,1)} %param.20) | copy-start | bytes 6291460
  (19 other events, 26.1 us)
Sparse Core Ops, SparseCore 0:
  9.5 33.8 all-gather.3
  49.9 72.8 all-gather.7
  125.5 75.8 all-gather.5
where the time goes:
time: 437 us; the launch traced here: 435 us
  waiting for transfers between devices  164 us (38%)
  matrix products  134 us (31%)
  other arithmetic  50.9 us (12%)
  local copies, waits for them, and re-layouts  50.6 us (12%)
  between operations  14.1 us (3%)
  loops' own time  11.9 us (3%)
  starting transfers between devices  4.99 us (1%)
    dot_general x16, matrix products, compute(): jnp.einsum('hmqk,khd->hmqd', probs.astype(jnp.bfloat16), value_block, pre...  73.1 us
    all_gather x1, waiting for transfers between devices, per_device(): key_piece = lax.all_gather(rk, 'sp', axis=0, tiled=True)  71 us
    all_gather x1, waiting for transfers between devices, per_device(): value_piece = lax.all_gather(values, 'sp', axis=0, tiled=True)  47.3 us
    dot_general x16, matrix products, compute(): jnp.einsum('hmqd,khmd->hmqk', rq, key_block, preferred_element_type=jnp.f...  40.7 us
    all_gather x1, waiting for transfers between devices, per_device(): projected = project(lax.all_gather(tokens, 'tp', axis=0, tiled=True))  35.5 us
    reduce_sum x16, other arithmetic, compute(): totals = totals * factor + jnp.sum(probs, axis=-1)  32.8 us
    cond x80, local copies, waits for them, and re-layouts  21.3 us
    dot_general x5, matrix products, project(): jnp.dot(normed, matrix, preferred_element_type=jnp.float32)  13.1 us
  transfers between devices with their start and end apart: 5, of which 5 were waited for; matrix products, arithmetic and copies ran while one was open for 6% of the time, Pallas kernels for 0%

commit v1 on v0

--- a/solution.py
+++ b/solution.py
@@ -92,7 +92,12 @@
     )
     carry = initial
     key_piece = lax.all_gather(rk, "sp", axis=0, tiled=True)
-    value_piece = lax.all_gather(values, "sp", axis=0, tiled=True)
+    ring = [values]
+    for hop in range(15):
+        ring.append(lax.ppermute(ring[-1], "sp", [(dev, (dev + 1) % 16) for dev in range(16)]))
+    value_piece = jnp.roll(
+        jnp.concatenate(ring[::-1], axis=0), (lax.axis_index("sp") + 1) * ring[0].shape[0], axis=0
+    )
     count = key_piece.shape[0]
     block = math.gcd(count, 512)
     blocks = count // block

time: 437 us -> 566 us (1.30)
  starting transfers between devices: 4.99 us -> 78.5 us
  local copies, waits for them, and re-layouts: 50.6 us -> 107 us
  waiting for transfers between devices: 164 us -> 155 us
    ppermute x0 -> x15, waiting for transfers between devices: none -> 110 us  [per_device(): lax.ppermute(ring[-1], 'sp', [(dev, (dev + 1) % 16) for dev in range(16)])]
    ppermute x0 -> x15, starting transfers between devices: none -> 73.6 us  [per_device(): lax.ppermute(ring[-1], 'sp', [(dev, (dev + 1) % 16) for dev in range(16)])]
    all_gather x1, waiting for transfers between devices: 71 us -> 0.01 us  [per_device(): key_piece = lax.all_gather(rk, 'sp', axis=0, tiled=True)]
    unnamed x31 -> x128, local copies, waits for them, and re-layouts: 7.74 us -> 55.6 us
    all_gather x1 -> x0, waiting for transfers between devices: 47.3 us -> none  [per_device(): value_piece = lax.all_gather(values, 'sp', axis=0, tiled=True)]
    dynamic_slice x0 -> x1, local copies, waits for them, and re-layouts: none -> 7.18 us  [per_device(): jnp.roll(jnp.concatenate(ring[::-1], axis=0), (lax.axis_index('sp') + 1)...]
  transfers between devices with their start and end apart: 5 -> 19, of which waited for: 5 -> 17; matrix products, arithmetic and copies ran while one was open for 6% -> 13% of each run, Pallas kernels for 0% -> 0%
where the time goes in v1:
time: 566 us; the launch traced here: 564 us
  waiting for transfers between devices  155 us (27%)
  matrix products  138 us (24%)
  local copies, waits for them, and re-layouts  107 us (19%)
  starting transfers between devices  78.5 us (14%)
  other arithmetic  54.5 us (10%)
  between operations  14.7 us (3%)
  loops' own time  12.4 us (2%)
    ppermute x15, waiting for transfers between devices, per_device(): lax.ppermute(ring[-1], 'sp', [(dev, (dev + 1) % 16) for dev in range(16)])  110 us
    ppermute x15, starting transfers between devices, per_device(): lax.ppermute(ring[-1], 'sp', [(dev, (dev + 1) % 16) for dev in range(16)])  73.6 us
    dot_general x16, matrix products, compute(): jnp.einsum('hmqk,khd->hmqd', probs.astype(jnp.bfloat16), value_block, pre...  73.1 us
    unnamed x128, local copies, waits for them, and re-layouts  55.6 us
    dot_general x16, matrix products, compute(): jnp.einsum('hmqd,khmd->hmqk', rq, key_block, preferred_element_type=jnp.f...  43 us
    all_gather x1, waiting for transfers between devices, per_device(): projected = project(lax.all_gather(tokens, 'tp', axis=0, tiled=True))  35.1 us
    reduce_sum x16, other arithmetic, compute(): totals = totals * factor + jnp.sum(probs, axis=-1)  32.8 us
    cond x80, local copies, waits for them, and re-layouts  21.4 us
  transfers between devices with their start and end apart: 19, of which 17 were waited for; matrix products, arithmetic and copies ran while one was open for 13% of the time, Pallas kernels for 0%

profile of v1, /device:TPU:29, one launch (start us, length us, event | category | flops | bytes accessed | tf_op | source)
XLA Modules:
  0.0 563.9 jit_solution(9157541417747441586)
XLA Ops:
  8.3 35.1 %all-gather.3.cloned.1.call-done = bf16[512,2048]{1,0:T(8,128)(2,1)} async-done(((bf16[256,2048]{1,0:T(8,128)(2,1)}), bf16[512,2048]{1,0:T(8,128)(2,1)}) %all-gather.3.cloned.1.call-update) | async-done | bytes 2097168 | tf_op jit(solution)/shard_map/all_gather | solution.py:71
  57.6 9.0 %collective-permute-done = bf16[512,4,128]{2,0,1:T(8,128)(2,1)S(1)} collective-permute-done((bf16[512,4,128]{2,0,1:T(8,128)(2,1)S(1)}, bf16[512,4,128]{2,0,1:T(8,128)(2,1)S(1)}, u32[]{:S(2)}, u32[]{:S(2)}) %collective-permute-start) | collective-permute-done | bytes 524320 | tf_op jit(solution)/shard_map/ppermute | solution.py:97
  71.8 16.9 %collective-permute-done.1 = bf16[512,4,128]{2,0,1:T(8,128)(2,1)S(1)} collective-permute-done((bf16[512,4,128]{2,0,1:T(8,128)(2,1)S(1)}, bf16[512,4,128]{2,0,1:T(8,128)(2,1)S(1)}, u32[]{:S(2)}, u32[]{:S(2)}) %collective-permute-start.1) | collective-permute-done | bytes 524320 | tf_op jit(solution)/shard_map/ppermute | solution.py:97
  94.7 16.6 %collective-permute-done.2 = bf16[512,4,128]{2,0,1:T(8,128)(2,1)S(1)} collective-permute-done((bf16[512,4,128]{2,0,1:T(8,128)(2,1)S(1)}, bf16[512,4,128]{2,0,1:T(8,128)(2,1)S(1)}, u32[]{:S(2)}, u32[]{:S(2)}) %collective-permute-start.2) | collective-permute-done | bytes 524320 | tf_op jit(solution)/shard_map/ppermute | solution.py:97
  117.2 15.8 %collective-permute-done.3 = bf16[512,4,128]{2,0,1:T(8,128)(2,1)S(1)} collective-permute-done((bf16[512,4,128]{2,0,1:T(8,128)(2,1)S(1)}, bf16[512,4,128]{2,0,1:T(8,128)(2,1)S(1)}, u32[]{:S(2)}, u32[]{:S(2)}) %collective-permute-start.3) | collective-permute-done | bytes 524320 | tf_op jit(solution)/shard_map/ppermute | solution.py:97
  139.0 6.9 %collective-permute-done.4 = bf16[512,4,128]{2,0,1:T(8,128)(2,1)S(1)} collective-permute-done((bf16[512,4,128]{2,0,1:T(8,128)(2,1)S(1)}, bf16[512,4,128]{2,0,1:T(8,128)(2,1)S(1)}, u32[]{:S(2)}, u32[]{:S(2)}) %collective-permute-start.4) | collective-permute-done | bytes 524320 | tf_op jit(solution)/shard_map/ppermute | solution.py:97
  151.8 6.1 %collective-permute-done.5 = bf16[512,4,128]{2,0,1:T(8,128)(2,1)S(1)} collective-permute-done((bf16[512,4,128]{2,0,1:T(8,128)(2,1)S(1)}, bf16[512,4,128]{2,0,1:T(8,128)(2,1)S(1)}, u32[]{:S(2)}, u32[]{:S(2)}) %collective-permute-start.5) | collective-permute-done | bytes 524320 | tf_op jit(solution)/shard_map/ppermute | solution.py:97
  163.9 6.1 %collective-permute-done.6 = bf16[512,4,128]{2,0,1:T(8,128)(2,1)S(1)} collective-permute-done((bf16[512,4,128]{2,0,1:T(8,128)(2,1)S(1)}, bf16[512,4,128]{2,0,1:T(8,128)(2,1)S(1)}, u32[]{:S(2)}, u32[]{:S(2)}) %collective-permute-start.6) | collective-permute-done | bytes 524320 | tf_op jit(solution)/shard_map/ppermute | solution.py:97
  176.0 6.1 %collective-permute-done.7 = bf16[512,4,128]{2,0,1:T(8,128)(2,1)S(1)} collective-permute-done((bf16[512,4,128]{2,0,1:T(8,128)(2,1)S(1)}, bf16[512,4,128]{2,0,1:T(8,128)(2,1)S(1)}, u32[]{:S(2)}, u32[]{:S(2)}) %collective-permute-start.7) | collective-permute-done | bytes 524320 | tf_op jit(solution)/shard_map/ppermute | solution.py:97
  200.2 6.1 %collective-permute-done.9 = bf16[512,4,128]{2,0,1:T(8,128)(2,1)S(1)} collective-permute-done((bf16[512,4,128]{2,0,1:T(8,128)(2,1)S(1)}, bf16[512,4,128]{2,0,1:T(8,128)(2,1)S(1)}, u32[]{:S(2)}, u32[]{:S(2)}) %collective-permute-start.9) | collective-permute-done | bytes 524320 | tf_op jit(solution)/shard_map/ppermute | solution.py:97
  311.2 7.2 %constant_dynamic-slice_fusion = bf16[8192,4,128]{2,0,1:T(8,128)(2,1)} fusion(bf16[16384,4,128]{2,0,1:T(8,128)(2,1)} %constant_dynamic-update-slice_fusion, s32[]{:T(128)S(6)} %select_n.25), kind=kLoop, calls=%fused_computation.180 | loop fusion | bytes 16777220 | tf_op jit(solution)/shard_map/jit(_roll_dynamic)/dynamic_slice | solution.py:98
  318.4 7.7 %copy.25 = bf16[16,512,4,128]{3,1,2,0:T(8,128)(2,1)} copy(bf16[16,512,4,128]{3,1,0,2:T(8,128)(2,1)} %bitcast.121) | data formatting | bytes 16777216
  326.1 8.0 %copy.53 = bf16[4,2,8,16,8,512]{5,4,2,1,0,3:T(8,128)(2,1)} copy(bf16[4,2,8,16,8,512]{5,4,3,2,1,0:T(8,128)(2,1)} %bitcast.124) | data formatting | bytes 16777216 | tf_op jit(solution)/shard_map/reshape | solution.py:104
  335.6 196.0 %while.15 = (s32[]{:T(128)}, f32[4,2,512]{2,1,0:T(2,128)S(1)}, f32[4,2,512]{2,1,0:T(2,128)S(1)}, f32[4,2,512,128]{3,2,1,0:T(8,128)}, s32[16]{0:T(128)S(1)}, /*in...) while((s32[]{:T(128)}, f32[4,2,512]{2,1,0:T(2,128)S(1)}, ...), condition=%wide.region_8.9_spmd.clone, body=%wide.region_3.8_spmd.clone.sunk | while | flops 833889280 | bytes 49034592 | solution.py:137
  337.1 11.0 %conditional.3 = ((f32[4,2,512]{2,1,0:T(2,128)S(1)}, f32[4,2,512]{2,1,0:T(2,128)S(1)}, f32[4,2,512,128]{3,2,1,0:T(8,128)})) conditional(s32[]{:T(128)} %convert_element_type.168, (f32[4,2,512]{2,1,0:T(2,128)S(1)}, f32[4,2,512]{2,1,0:T(2,128)S(1)}, f32[4,2,512,128]{3,2,1,0:T(8,128)}) %tuple.88, (s32[]{:T(128)}, s32[]{:T(128)}, ...), branch_computations={%region_4.4_spmd, %region_5.7_spmd} | conditional | flops 833889280 | bytes 49032288 | solution.py:135
  349.3 11.0 %conditional.3 = ((f32[4,2,512]{2,1,0:T(2,128)S(1)}, f32[4,2,512]{2,1,0:T(2,128)S(1)}, f32[4,2,512,128]{3,2,1,0:T(8,128)})) conditional(s32[]{:T(128)} %convert_element_type.168, (f32[4,2,512]{2,1,0:T(2,128)S(1)}, f32[4,2,512]{2,1,0:T(2,128)S(1)}, f32[4,2,512,128]{3,2,1,0:T(8,128)}) %tuple.88, (s32[]{:T(128)}, s32[]{:T(128)}, ...), branch_computations={%region_4.4_spmd, %region_5.7_spmd} | conditional | flops 833889280 | bytes 49032288 | solution.py:135
  361.6 11.0 %conditional.3 = ((f32[4,2,512]{2,1,0:T(2,128)S(1)}, f32[4,2,512]{2,1,0:T(2,128)S(1)}, f32[4,2,512,128]{3,2,1,0:T(8,128)})) conditional(s32[]{:T(128)} %convert_element_type.168, (f32[4,2,512]{2,1,0:T(2,128)S(1)}, f32[4,2,512]{2,1,0:T(2,128)S(1)}, f32[4,2,512,128]{3,2,1,0:T(8,128)}) %tuple.88, (s32[]{:T(128)}, s32[]{:T(128)}, ...), branch_computations={%region_4.4_spmd, %region_5.7_spmd} | conditional | flops 833889280 | bytes 49032288 | solution.py:135
  373.8 11.0 %conditional.3 = ((f32[4,2,512]{2,1,0:T(2,128)S(1)}, f32[4,2,512]{2,1,0:T(2,128)S(1)}, f32[4,2,512,128]{3,2,1,0:T(8,128)})) conditional(s32[]{:T(128)} %convert_element_type.168, (f32[4,2,512]{2,1,0:T(2,128)S(1)}, f32[4,2,512]{2,1,0:T(2,128)S(1)}, f32[4,2,512,128]{3,2,1,0:T(8,128)}) %tuple.88, (s32[]{:T(128)}, s32[]{:T(128)}, ...), branch_computations={%region_4.4_spmd, %region_5.7_spmd} | conditional | flops 833889280 | bytes 49032288 | solution.py:135
  386.0 11.0 %conditional.3 = ((f32[4,2,512]{2,1,0:T(2,128)S(1)}, f32[4,2,512]{2,1,0:T(2,128)S(1)}, f32[4,2,512,128]{3,2,1,0:T(8,128)})) conditional(s32[]{:T(128)} %convert_element_type.168, (f32[4,2,512]{2,1,0:T(2,128)S(1)}, f32[4,2,512]{2,1,0:T(2,128)S(1)}, f32[4,2,512,128]{3,2,1,0:T(8,128)}) %tuple.88, (s32[]{:T(128)}, s32[]{:T(128)}, ...), branch_computations={%region_4.4_spmd, %region_5.7_spmd} | conditional | flops 833889280 | bytes 49032288 | solution.py:135
  398.3 11.0 %conditional.3 = ((f32[4,2,512]{2,1,0:T(2,128)S(1)}, f32[4,2,512]{2,1,0:T(2,128)S(1)}, f32[4,2,512,128]{3,2,1,0:T(8,128)})) conditional(s32[]{:T(128)} %convert_element_type.168, (f32[4,2,512]{2,1,0:T(2,128)S(1)}, f32[4,2,512]{2,1,0:T(2,128)S(1)}, f32[4,2,512,128]{3,2,1,0:T(8,128)}) %tuple.88, (s32[]{:T(128)}, s32[]{:T(128)}, ...), branch_computations={%region_4.4_spmd, %region_5.7_spmd} | conditional | flops 833889280 | bytes 49032288 | solution.py:135
  410.5 11.0 %conditional.3 = ((f32[4,2,512]{2,1,0:T(2,128)S(1)}, f32[4,2,512]{2,1,0:T(2,128)S(1)}, f32[4,2,512,128]{3,2,1,0:T(8,128)})) conditional(s32[]{:T(128)} %convert_element_type.168, (f32[4,2,512]{2,1,0:T(2,128)S(1)}, f32[4,2,512]{2,1,0:T(2,128)S(1)}, f32[4,2,512,128]{3,2,1,0:T(8,128)}) %tuple.88, (s32[]{:T(128)}, s32[]{:T(128)}, ...), branch_computations={%region_4.4_spmd, %region_5.7_spmd} | conditional | flops 833889280 | bytes 49032288 | solution.py:135
  422.7 11.0 %conditional.3 = ((f32[4,2,512]{2,1,0:T(2,128)S(1)}, f32[4,2,512]{2,1,0:T(2,128)S(1)}, f32[4,2,512,128]{3,2,1,0:T(8,128)})) conditional(s32[]{:T(128)} %convert_element_type.168, (f32[4,2,512]{2,1,0:T(2,128)S(1)}, f32[4,2,512]{2,1,0:T(2,128)S(1)}, f32[4,2,512,128]{3,2,1,0:T(8,128)}) %tuple.88, (s32[]{:T(128)}, s32[]{:T(128)}, ...), branch_computations={%region_4.4_spmd, %region_5.7_spmd} | conditional | flops 833889280 | bytes 49032288 | solution.py:135
  435.0 11.0 %conditional.3 = ((f32[4,2,512]{2,1,0:T(2,128)S(1)}, f32[4,2,512]{2,1,0:T(2,128)S(1)}, f32[4,2,512,128]{3,2,1,0:T(8,128)})) conditional(s32[]{:T(128)} %convert_element_type.168, (f32[4,2,512]{2,1,0:T(2,128)S(1)}, f32[4,2,512]{2,1,0:T(2,128)S(1)}, f32[4,2,512,128]{3,2,1,0:T(8,128)}) %tuple.88, (s32[]{:T(128)}, s32[]{:T(128)}, ...), branch_computations={%region_4.4_spmd, %region_5.7_spmd} | conditional | flops 833889280 | bytes 49032288 | solution.py:135
  447.2 11.0 %conditional.3 = ((f32[4,2,512]{2,1,0:T(2,128)S(1)}, f32[4,2,512]{2,1,0:T(2,128)S(1)}, f32[4,2,512,128]{3,2,1,0:T(8,128)})) conditional(s32[]{:T(128)} %convert_element_type.168, (f32[4,2,512]{2,1,0:T(2,128)S(1)}, f32[4,2,512]{2,1,0:T(2,128)S(1)}, f32[4,2,512,128]{3,2,1,0:T(8,128)}) %tuple.88, (s32[]{:T(128)}, s32[]{:T(128)}, ...), branch_computations={%region_4.4_spmd, %region_5.7_spmd} | conditional | flops 833889280 | bytes 49032288 | solution.py:135
  459.4 11.0 %conditional.3 = ((f32[4,2,512]{2,1,0:T(2,128)S(1)}, f32[4,2,512]{2,1,0:T(2,128)S(1)}, f32[4,2,512,128]{3,2,1,0:T(8,128)})) conditional(s32[]{:T(128)} %convert_element_type.168, (f32[4,2,512]{2,1,0:T(2,128)S(1)}, f32[4,2,512]{2,1,0:T(2,128)S(1)}, f32[4,2,512,128]{3,2,1,0:T(8,128)}) %tuple.88, (s32[]{:T(128)}, s32[]{:T(128)}, ...), branch_computations={%region_4.4_spmd, %region_5.7_spmd} | conditional | flops 833889280 | bytes 49032288 | solution.py:135
  471.7 11.0 %conditional.3 = ((f32[4,2,512]{2,1,0:T(2,128)S(1)}, f32[4,2,512]{2,1,0:T(2,128)S(1)}, f32[4,2,512,128]{3,2,1,0:T(8,128)})) conditional(s32[]{:T(128)} %convert_element_type.168, (f32[4,2,512]{2,1,0:T(2,128)S(1)}, f32[4,2,512]{2,1,0:T(2,128)S(1)}, f32[4,2,512,128]{3,2,1,0:T(8,128)}) %tuple.88, (s32[]{:T(128)}, s32[]{:T(128)}, ...), branch_computations={%region_4.4_spmd, %region_5.7_spmd} | conditional | flops 833889280 | bytes 49032288 | solution.py:135
  483.9 11.0 %conditional.3 = ((f32[4,2,512]{2,1,0:T(2,128)S(1)}, f32[4,2,512]{2,1,0:T(2,128)S(1)}, f32[4,2,512,128]{3,2,1,0:T(8,128)})) conditional(s32[]{:T(128)} %convert_element_type.168, (f32[4,2,512]{2,1,0:T(2,128)S(1)}, f32[4,2,512]{2,1,0:T(2,128)S(1)}, f32[4,2,512,128]{3,2,1,0:T(8,128)}) %tuple.88, (s32[]{:T(128)}, s32[]{:T(128)}, ...), branch_computations={%region_4.4_spmd, %region_5.7_spmd} | conditional | flops 833889280 | bytes 49032288 | solution.py:135
  496.1 11.0 %conditional.3 = ((f32[4,2,512]{2,1,0:T(2,128)S(1)}, f32[4,2,512]{2,1,0:T(2,128)S(1)}, f32[4,2,512,128]{3,2,1,0:T(8,128)})) conditional(s32[]{:T(128)} %convert_element_type.168, (f32[4,2,512]{2,1,0:T(2,128)S(1)}, f32[4,2,512]{2,1,0:T(2,128)S(1)}, f32[4,2,512,128]{3,2,1,0:T(8,128)}) %tuple.88, (s32[]{:T(128)}, s32[]{:T(128)}, ...), branch_computations={%region_4.4_spmd, %region_5.7_spmd} | conditional | flops 833889280 | bytes 49032288 | solution.py:135
  508.4 11.0 %conditional.3 = ((f32[4,2,512]{2,1,0:T(2,128)S(1)}, f32[4,2,512]{2,1,0:T(2,128)S(1)}, f32[4,2,512,128]{3,2,1,0:T(8,128)})) conditional(s32[]{:T(128)} %convert_element_type.168, (f32[4,2,512]{2,1,0:T(2,128)S(1)}, f32[4,2,512]{2,1,0:T(2,128)S(1)}, f32[4,2,512,128]{3,2,1,0:T(8,128)}) %tuple.88, (s32[]{:T(128)}, s32[]{:T(128)}, ...), branch_computations={%region_4.4_spmd, %region_5.7_spmd} | conditional | flops 833889280 | bytes 49032288 | solution.py:135
  520.6 11.0 %conditional.3 = ((f32[4,2,512]{2,1,0:T(2,128)S(1)}, f32[4,2,512]{2,1,0:T(2,128)S(1)}, f32[4,2,512,128]{3,2,1,0:T(8,128)})) conditional(s32[]{:T(128)} %convert_element_type.168, (f32[4,2,512]{2,1,0:T(2,128)S(1)}, f32[4,2,512]{2,1,0:T(2,128)S(1)}, f32[4,2,512,128]{3,2,1,0:T(8,128)}) %tuple.88, (s32[]{:T(128)}, s32[]{:T(128)}, ...), branch_computations={%region_4.4_spmd, %region_5.7_spmd} | conditional | flops 833889280 | bytes 49032288 | solution.py:135
  540.3 7.6 %all-to-all-done = bf16[2,256,1024]{2,1,0:T(8,128)(2,1)S(1)} async-done(((bf16[2,256,1024]{2,1,0:T(8,128)(2,1)}), bf16[2,256,1024]{2,1,0:T(8,128)(2,1)S(1)}, u32[]{:S(2)}, u32[]{:S(2)}) %all-to-all-start) | async-done | bytes 1048608 | tf_op jit(solution)/shard_map/all_to_all | solution.py:175
  550.3 6.7 %fusion.23 = bf16[256,2048]{1,0:T(8,128)(2,1)} fusion(bf16[2,2,512,2048]{3,2,1,0:T(8,128)(2,1)} %bitcast.123, bf16[256,2,2,512]{0,3,2,1:T(8,128)(2,1)S(1)} %bitcast.126), kind=kOutput, calls=%fused_computation.31 | convolution fusion | flops 2148007936 | bytes 10485760 | tf_op jit(solution)/shard_map/rtcj,ctjd->rd/dot_general | solution.py:177
  (418 shorter events, 375.0 us)
Async XLA Ops:
  7.2 38.5 %copy-start = (bf16[2048,512]{1,0:T(8,128)(2,1)S(1)}, bf16[2048,512]{1,0:T(8,128)(2,1)}, u32[]{:S(2)}) copy-start(bf16[2048,512]{1,0:T(8,128)(2,1)} %param.20) | copy-start | bytes 6291460
  7.2 41.5 %copy-start.48 = (f32[2048]{0:T(1024)S(1)}, f32[2048]{0:T(1024)}, u32[]{:S(2)}) copy-start(f32[2048]{0:T(1024)} %param.19) | copy-start | bytes 24580
  7.2 36.2 %all-gather.3.cloned.1.call-start = ((), (), s32[]{:S(2)}) async-start(), calls=%async_computation.1 | async-start | bytes 3145728 | tf_op jit(solution)/shard_map/all_gather | solution.py:71
  7.9 318.2 %all-gather.5.cloned.1.call-start = ((), (), s32[]{:S(2)}) async-start(), calls=%async_computation.2 | async-start | bytes 8912896 | tf_op jit(solution)/shard_map/all_gather | solution.py:94
  50.2 174.2 %copy-start.29 = (f32[31,512]{1,0:T(8,128)S(1)}, f32[31,512]{1,0:T(8,128)}, u32[]{:S(2)}) copy-start(f32[31,512]{1,0:T(8,128)} %param.28) | copy-start | bytes 190468
  52.5 194.9 %copy-start.6 = (bf16[512,2048]{1,0:T(8,128)(2,1)S(1)}, bf16[512,2048]{1,0:T(8,128)(2,1)}, u32[]{:S(2)}) copy-start(bf16[512,2048]{1,0:T(8,128)(2,1)} %all-gather.3.cloned.1.call-done) | copy-start | bytes 6291460
  56.6 10.0 %collective-permute-start = (bf16[512,4,128]{2,0,1:T(8,128)(2,1)S(1)}, bf16[512,4,128]{2,0,1:T(8,128)(2,1)S(1)}, u32[]{:S(2)}, u32[]{:S(2)}) collective-permute-start(bf16[512,4,128]{2,0,1:T(8,128)(2,1)S(1)} %copy.21), channel_id=1, source_target_pairs={{0,2},{2,4},{4,6},{6,8},{8,10},{10,12},{12,14},{14,16},{16,18},{18... | collective-permute-start | bytes 1572872 | tf_op jit(solution)/shard_map/ppermute | solution.py:97
  66.6 22.1 %collective-permute-start.1 = (bf16[512,4,128]{2,0,1:T(8,128)(2,1)S(1)}, bf16[512,4,128]{2,0,1:T(8,128)(2,1)S(1)}, u32[]{:S(2)}, u32[]{:S(2)}) collective-permute-start(bf16[512,4,128]{2,0,1:T(8,128)(2,1)S(1)} %collective-permute-done), channel_id=1, source_target_pairs={{0,2},{2,4},{4,6},{6,8},{8,10},{10,12},{12,14},{14,16},{16,18},{18... | collective-permute-start | bytes 1572872 | tf_op jit(solution)/shard_map/ppermute | solution.py:97
  89.5 21.8 %collective-permute-start.2 = (bf16[512,4,128]{2,0,1:T(8,128)(2,1)S(1)}, bf16[512,4,128]{2,0,1:T(8,128)(2,1)S(1)}, u32[]{:S(2)}, u32[]{:S(2)}) collective-permute-start(bf16[512,4,128]{2,0,1:T(8,128)(2,1)S(1)} %collective-permute-done.1), channel_id=1, source_target_pairs={{0,2},{2,4},{4,6},{6,8},{8,10},{10,12},{12,14},{14,16},{16,18},{18... | collective-permute-start | bytes 1572872 | tf_op jit(solution)/shard_map/ppermute | solution.py:97
  112.0 20.9 %collective-permute-start.3 = (bf16[512,4,128]{2,0,1:T(8,128)(2,1)S(1)}, bf16[512,4,128]{2,0,1:T(8,128)(2,1)S(1)}, u32[]{:S(2)}, u32[]{:S(2)}) collective-permute-start(bf16[512,4,128]{2,0,1:T(8,128)(2,1)S(1)} %collective-permute-done.2), channel_id=1, source_target_pairs={{0,2},{2,4},{4,6},{6,8},{8,10},{10,12},{12,14},{14,16},{16,18},{18... | collective-permute-start | bytes 1572872 | tf_op jit(solution)/shard_map/ppermute | solution.py:97
  133.8 12.1 %collective-permute-start.4 = (bf16[512,4,128]{2,0,1:T(8,128)(2,1)S(1)}, bf16[512,4,128]{2,0,1:T(8,128)(2,1)S(1)}, u32[]{:S(2)}, u32[]{:S(2)}) collective-permute-start(bf16[512,4,128]{2,0,1:T(8,128)(2,1)S(1)} %collective-permute-done.3), channel_id=1, source_target_pairs={{0,2},{2,4},{4,6},{6,8},{8,10},{10,12},{12,14},{14,16},{16,18},{18... | collective-permute-start | bytes 1572872 | tf_op jit(solution)/shard_map/ppermute | solution.py:97
  146.6 11.3 %collective-permute-start.5 = (bf16[512,4,128]{2,0,1:T(8,128)(2,1)S(1)}, bf16[512,4,128]{2,0,1:T(8,128)(2,1)S(1)}, u32[]{:S(2)}, u32[]{:S(2)}) collective-permute-start(bf16[512,4,128]{2,0,1:T(8,128)(2,1)S(1)} %collective-permute-done.4), channel_id=1, source_target_pairs={{0,2},{2,4},{4,6},{6,8},{8,10},{10,12},{12,14},{14,16},{16,18},{18... | collective-permute-start | bytes 1572872 | tf_op jit(solution)/shard_map/ppermute | solution.py:97
  158.8 11.3 %collective-permute-start.6 = (bf16[512,4,128]{2,0,1:T(8,128)(2,1)S(1)}, bf16[512,4,128]{2,0,1:T(8,128)(2,1)S(1)}, u32[]{:S(2)}, u32[]{:S(2)}) collective-permute-start(bf16[512,4,128]{2,0,1:T(8,128)(2,1)S(1)} %collective-permute-done.5), channel_id=1, source_target_pairs={{0,2},{2,4},{4,6},{6,8},{8,10},{10,12},{12,14},{14,16},{16,18},{18... | collective-permute-start | bytes 1572872 | tf_op jit(solution)/shard_map/ppermute | solution.py:97
  170.9 11.3 %collective-permute-start.7 = (bf16[512,4,128]{2,0,1:T(8,128)(2,1)S(1)}, bf16[512,4,128]{2,0,1:T(8,128)(2,1)S(1)}, u32[]{:S(2)}, u32[]{:S(2)}) collective-permute-start(bf16[512,4,128]{2,0,1:T(8,128)(2,1)S(1)} %collective-permute-done.6), channel_id=1, source_target_pairs={{0,2},{2,4},{4,6},{6,8},{8,10},{10,12},{12,14},{14,16},{16,18},{18... | collective-permute-start | bytes 1572872 | tf_op jit(solution)/shard_map/ppermute | solution.py:97
  183.0 11.3 %collective-permute-start.8 = (bf16[512,4,128]{2,0,1:T(8,128)(2,1)S(1)}, bf16[512,4,128]{2,0,1:T(8,128)(2,1)S(1)}, u32[]{:S(2)}, u32[]{:S(2)}) collective-permute-start(bf16[512,4,128]{2,0,1:T(8,128)(2,1)S(1)} %collective-permute-done.7), channel_id=1, source_target_pairs={{0,2},{2,4},{4,6},{6,8},{8,10},{10,12},{12,14},{14,16},{16,18},{18... | collective-permute-start | bytes 1572872 | tf_op jit(solution)/shard_map/ppermute | solution.py:97
  195.0 11.3 %collective-permute-start.9 = (bf16[512,4,128]{2,0,1:T(8,128)(2,1)S(1)}, bf16[512,4,128]{2,0,1:T(8,128)(2,1)S(1)}, u32[]{:S(2)}, u32[]{:S(2)}) collective-permute-start(bf16[512,4,128]{2,0,1:T(8,128)(2,1)S(1)} %collective-permute-done.8), channel_id=1, source_target_pairs={{0,2},{2,4},{4,6},{6,8},{8,10},{10,12},{12,14},{14,16},{16,18},{18... | collective-permute-start | bytes 1572872 | tf_op jit(solution)/shard_map/ppermute | solution.py:97
  207.1 11.3 %collective-permute-start.10 = (bf16[512,4,128]{2,0,1:T(8,128)(2,1)S(1)}, bf16[512,4,128]{2,0,1:T(8,128)(2,1)S(1)}, u32[]{:S(2)}, u32[]{:S(2)}) collective-permute-start(bf16[512,4,128]{2,0,1:T(8,128)(2,1)S(1)} %collective-permute-done.9), channel_id=1, source_target_pairs={{0,2},{2,4},{4,6},{6,8},{8,10},{10,12},{12,14},{14,16},{16,18},{18... | collective-permute-start | bytes 1572872 | tf_op jit(solution)/shard_map/ppermute | solution.py:97
  219.2 11.3 %collective-permute-start.11 = (bf16[512,4,128]{2,0,1:T(8,128)(2,1)S(1)}, bf16[512,4,128]{2,0,1:T(8,128)(2,1)}, u32[]{:S(2)}, u32[]{:S(2)}) collective-permute-start(bf16[512,4,128]{2,0,1:T(8,128)(2,1)S(1)} %collective-permute-done.10), channel_id=1, source_target_pairs={{0,2},{2,4},{4,6},{6,8},{8,10},{10,12},{12,14},{14,16},{16,18},{18... | collective-permute-start | bytes 1572872 | tf_op jit(solution)/shard_map/ppermute | solution.py:97
  230.6 11.7 %collective-permute-start.12 = (bf16[512,4,128]{2,0,1:T(8,128)(2,1)}, bf16[512,4,128]{2,0,1:T(8,128)(2,1)}, u32[]{:S(2)}, u32[]{:S(2)}) collective-permute-start(bf16[512,4,128]{2,0,1:T(8,128)(2,1)} %collective-permute-done.11), channel_id=1, source_target_pairs={{0,2},{2,4},{4,6},{6,8},{8,10},{10,12},{12,14},{14,16},{16,18},{18... | collective-permute-start | bytes 1572872 | tf_op jit(solution)/shard_map/ppermute | solution.py:97
  242.3 11.6 %collective-permute-start.13 = (bf16[512,4,128]{2,0,1:T(8,128)(2,1)}, bf16[512,4,128]{2,0,1:T(8,128)(2,1)}, u32[]{:S(2)}, u32[]{:S(2)}) collective-permute-start(bf16[512,4,128]{2,0,1:T(8,128)(2,1)} %collective-permute-done.12), channel_id=1, source_target_pairs={{0,2},{2,4},{4,6},{6,8},{8,10},{10,12},{12,14},{14,16},{16,18},{18... | collective-permute-start | bytes 1572872 | tf_op jit(solution)/shard_map/ppermute | solution.py:97
  250.6 3.1 collective-permute-start.15
  253.9 17.6 %collective-permute-start.14 = (bf16[512,4,128]{2,0,1:T(8,128)(2,1)}, bf16[512,4,128]{2,0,1:T(8,128)(2,1)}, u32[]{:S(2)}, u32[]{:S(2)}) collective-permute-start(bf16[512,4,128]{2,0,1:T(8,128)(2,1)} %collective-permute-done.13), channel_id=1, source_target_pairs={{0,2},{2,4},{4,6},{6,8},{8,10},{10,12},{12,14},{14,16},{16,18},{18... | collective-permute-start | bytes 1572872 | tf_op jit(solution)/shard_map/ppermute | solution.py:97
  264.9 23.7 %copy-start.12 = (bf16[512,4,128]{2,0,1:T(8,128)(2,1)S(1)}, bf16[512,4,128]{2,0,1:T(8,128)(2,1)}, u32[]{:S(2)}) copy-start(bf16[512,4,128]{2,0,1:T(8,128)(2,1)} %copy-done.11) | copy-start | bytes 1572868
  264.9 24.6 %copy-start.10 = (bf16[512,4,128]{2,0,1:T(8,128)(2,1)S(1)}, bf16[512,4,128]{2,0,1:T(8,128)(2,1)}, u32[]{:S(2)}) copy-start(bf16[512,4,128]{2,0,1:T(8,128)(2,1)} %copy-done.9) | copy-start | bytes 1572868
  265.0 25.4 %copy-start.8 = (bf16[512,4,128]{2,0,1:T(8,128)(2,1)S(1)}, bf16[512,4,128]{2,0,1:T(8,128)(2,1)}, u32[]{:S(2)}) copy-start(bf16[512,4,128]{2,0,1:T(8,128)(2,1)} %copy-done.7) | copy-start | bytes 1572868
  279.2 21.5 %copy-start.27 = (bf16[512,4,128]{2,0,1:T(8,128)(2,1)S(1)}, bf16[512,4,128]{2,0,1:T(8,128)(2,1)}, u32[]{:S(2)}) copy-start(bf16[512,4,128]{2,0,1:T(8,128)(2,1)} %copy-done.26) | copy-start | bytes 1572868
  281.2 20.4 %copy-start.24 = (bf16[512,4,128]{2,0,1:T(8,128)(2,1)S(1)}, bf16[512,4,128]{2,0,1:T(8,128)(2,1)}, u32[]{:S(2)}) copy-start(bf16[512,4,128]{2,0,1:T(8,128)(2,1)} %copy-done.23) | copy-start | bytes 1572868
  335.6 196.1 %copy-start.46 = (f32[4]{0:T(128)S(1)}, f32[4]{0:T(128)}, u32[]{:S(2)}) copy-start(f32[4]{0:T(128)} %param.26) | copy-start | bytes 52
  335.6 198.3 %copy-start.45 = (f32[128]{0:T(128)S(1)}, f32[128]{0:T(128)}, u32[]{:S(2)}) copy-start(f32[128]{0:T(128)} %param.27) | copy-start | bytes 1540
  335.6 199.3 %copy-start.25 = (bf16[512,512]{1,0:T(8,128)(2,1)S(1)}, bf16[512,512]{1,0:T(8,128)(2,1)}, u32[]{:S(2)}) copy-start(bf16[512,512]{1,0:T(8,128)(2,1)} %multiply_convert_fusion) | copy-start | bytes 1572868
  534.9 22.1 %copy-start.1 = (bf16[2048,512]{1,0:T(8,128)(2,1)S(1)}, bf16[2048,512]{1,0:T(8,128)(2,1)}, u32[]{:S(2)}) copy-start(bf16[2048,512]{1,0:T(8,128)(2,1)} %param.20) | copy-start | bytes 6291460
  536.0 11.8 %all-to-all-start = ((bf16[2,256,1024]{2,1,0:T(8,128)(2,1)}), bf16[2,256,1024]{2,1,0:T(8,128)(2,1)S(1)}, u32[]{:S(2)}, u32[]{:S(2)}) async-start(bf16[2,256,1024]{2,1,0:T(8,128)(2,1)} %pad_maximum_fusion), calls=%async_computation | async-start | bytes 2097152 | tf_op jit(solution)/shard_map/all_to_all | solution.py:175
  (66 other events, 459.6 us)
Sparse Core Ops, SparseCore 0:
  9.5 33.8 all-gather.2
  52.7 91.2 all-gather.4
